TPU v7x, 256 devices: a whole 4x4x8 slice. The times are simulated.
256 devices in a mesh: sp: 32 (over z, y), tp: 8 (over x, core).
Axes of the slice: x: 4, y: 4, z: 8, core: 2. Of those that a mesh axis runs over, the one named last changes fastest.
Arguments:
- stream: bfloat16 [8192, 2048], P('sp'), may hold values from -3 to 3
- first_group_queries: bfloat16 [8192, 512], P('sp', 'tp'), may hold values from -6 to 6
- first_group_keys: bfloat16 [8192, 512], P('sp', 'tp'), may hold values from -6 to 6
- first_group_values: bfloat16 [8192, 1024], P('sp', 'tp'), may hold values from -5.5 to 5.5
- first_gate_logits: bfloat16 [8192, 1024], P('sp', 'tp'), may hold values from -6 to 6
- first_decay_logits: bfloat16 [8192, 512], P('sp', 'tp'), may hold values from -4.75 to 14.5
- second_group_queries: bfloat16 [8192, 1024], P('sp', 'tp'), may hold values from -6 to 6
- second_group_keys: bfloat16 [8192, 1024], P('sp', 'tp'), may hold values from -6 to 6
- second_group_values: bfloat16 [8192, 1024], P('sp', 'tp'), may hold values from -5.5 to 5.5
- second_gate_logits: bfloat16 [8192, 1024], P('sp', 'tp'), may hold values from -6 to 6
- second_decay_logits: bfloat16 [8192, 1024], P('sp', 'tp'), may hold values from -4.75 to 14.5
- position_log_decay: float32 [8192], P('sp'), may hold values from -0.6932 to 0, as said below
- per_head_norm_gain: float32 [128], replicated, may hold values from 0.1 to 1.9
- first_output_weight: bfloat16 [1024, 2048], P('tp'), may hold values from -0.125 to 0.125
- second_output_weight: bfloat16 [1024, 2048], P('tp'), may hold values from -0.125 to 0.125
- feedforward_norm_gain: float32 [2048], replicated, may hold values from 0.1 to 1.9
- gate_weight: bfloat16 [2048, 5632], P('sp', 'tp'), may hold values from -0.125 to 0.125
- up_weight: bfloat16 [2048, 5632], P('sp', 'tp'), may hold values from -0.125 to 0.125
- down_weight: bfloat16 [5632, 2048], P('tp', 'sp'), may hold values from -0.078125 to 0.078125
Outputs:
- refined: bfloat16 [8192, 2048], P(('sp', 'tp'))
Inputs may be any that keep to these rules, and one draw needn't show every extreme that they name: `position_log_decay`: most positions carry 0.
All inputs are finite; a program needn't handle non-finite values.
Results may differ from a plain program's by a relative error of at most 0.018.
Values may be sent and summed in bfloat16 or wider, within the bound.
No kernel may reach another device: no remote copies, remote signals or barrier semaphores. Data moves between devices by JAX's collectives and lax.ppermute only.
A program may use at most 64 MiB of HBM per device.

v0:
```python
import jax
import jax.numpy as jnp
from jax import lax
from jax.sharding import Mesh
from jax.sharding import PartitionSpec as P

KEY_SIZE_FIRST = 64
KEY_SIZE_SECOND = 128
DV = 128
BLK = 64
SP = ("sp_0", "sp_1")
SP_TP = ("sp_0", "sp_1", "tp")


decay_softness = 16.0
norm_eps = 1e-06


def filled_with(value, identity):
    return jax.tree.map(
        lambda part, zero: jnp.zeros_like(part) + jnp.asarray(zero, part.dtype), value, identity
    )


def gathered_once(value, axis):
    leaves = jax.tree.leaves(value)
    sequence = sorted(range(len(leaves)), key=lambda k: -leaves[k].size)
    width = (1, *leaves[sequence[0]].shape)[-1]
    lines = [
        jnp.pad(leaves[k].reshape(-1), (0, -leaves[k].size % width)).reshape(-1, width)
        for k in sequence
    ]
    both, at, found = (lax.all_gather(jnp.concatenate(lines), axis), 0, {})
    for k, line in zip(sequence, lines):
        section = both[:, at : at + len(line)].reshape(len(both), -1)
        found[k] = section[:, : leaves[k].size].reshape(-1, *leaves[k].shape)
        at += len(line)
    numbers = iter(range(len(leaves)))
    return jax.tree.map(lambda _: found[next(numbers)], value)


def carried_in(value, axes, combine, identity, reverse):
    before = start = filled_with(value, identity)
    running = value
    for axis in reversed(axes):
        size, index = (lax.axis_size(axis), lax.axis_index(axis))
        pieces = gathered_once(
            jax.tree.map(
                lambda part, kind: part.astype(kind),
                running,
                (jnp.bfloat16, jnp.bfloat16, jnp.bfloat16, jnp.bfloat16),
            ),
            axis,
        )
        inside, running = (start, start)
        for k in reversed(range(size)) if reverse else range(size):
            passed = k > index if reverse else k < index
            running = combine(
                running, jax.tree.map(lambda part, own: part[k].astype(own.dtype), pieces, value)
            )
            inside = jax.tree.map(lambda new, old: jnp.where(passed, new, old), running, inside)
        before = combine(inside, before)
    return before


def cut_along(value, dim, size):
    before, after = (value.shape[:dim], value.shape[dim + 1 :])
    return jnp.moveaxis(value.reshape(*before, size, -1, *after), dim, 0)


def summed_on_arrival(value, axis, dim):
    size = lax.axis_size(axis)
    blocks = lax.all_to_all(cut_along(value, dim, size), axis, 0, 0, tiled=True)
    return jnp.sum(blocks.astype(jnp.float32), axis=0)


def copy_for_each(value, axis):
    size = lax.axis_size(axis)
    return lax.all_to_all(
        jnp.broadcast_to(value[None], (size, *value.shape)), axis, 0, 0, tiled=True
    )


def in_order(blocks, dim):
    blocks = jnp.moveaxis(blocks, 0, dim)
    lengths = blocks.shape
    return blocks.reshape(*lengths[:dim], lengths[dim] * lengths[dim + 1], *lengths[dim + 2 :])


def collect(value, axis, dim):
    blocks = copy_for_each(value, axis)
    return in_order(blocks, dim)


def side_by_side(arrays, axis, dim, along):
    widths = [a.shape[along] for a in arrays]
    both = jnp.concatenate(arrays, axis=along)
    result = lax.all_gather(both, axis, axis=dim, tiled=True)
    return tuple(jnp.split(result, [sum(widths[:k]) for k in range(1, len(widths))], axis=along))


def gather_axes(value, axes, dim):
    for axis in reversed(axes):
        value = lax.all_gather(value, axis, axis=dim, tiled=True)
    return value


def channel_log_decays(decay_logits, position_log_decay, key_channels):
    channel_log_decay = (
        jax.nn.log_sigmoid(decay_logits.astype(jnp.float32)) / decay_softness
        + position_log_decay[:, None]
    )
    return channel_log_decay.reshape(decay_logits.shape[0], -1, key_channels)


def one_way(query_matrix, key_matrix, value_matrix, channel_log_decay, start_state):
    length, heads, key_channels = query_matrix.shape
    value_width = value_matrix.shape[-1]
    block_count = length // BLK

    def blocks(member):
        return member.reshape(block_count, BLK, heads, member.shape[-1]).transpose(0, 2, 1, 3)

    query_blocks = blocks(query_matrix)
    key_blocks = blocks(key_matrix)
    value_blocks = blocks(value_matrix)
    running = jnp.cumsum(blocks(channel_log_decay), axis=2)
    block_last = running[:, :, -1:, :]
    query_in = query_blocks * jnp.exp(running)
    key_in = key_blocks * jnp.exp(-running)
    key_end = key_blocks * jnp.exp(block_last - running)
    places = jnp.arange(BLK, dtype=jnp.int32)
    lower = places[:, None] >= places[None, :]
    scores = jnp.where(lower, jnp.einsum("nhid,nhjd->nhij", query_in, key_in), 0.0)
    local_out = jnp.einsum("nhij,nhjv->nhiv", scores, value_blocks)

    def advance(states, inputs):
        query_part, key_part, value_part, last_part = inputs
        emitted = jnp.einsum("hid,hdv->hiv", query_part, states)
        states = states * jnp.exp(last_part)[:, 0, :, None] + jnp.einsum(
            "hjd,hjv->hdv", key_part, value_part
        )
        return (states, emitted)

    _, carried = lax.scan(advance, start_state, (query_in, key_end, value_blocks, block_last))
    return (local_out + carried).transpose(0, 2, 1, 3).reshape(length, heads, value_width)


def prepare_inputs(
    query_matrix, key_matrix, value_matrix, decay_logits, position_log_decay, key_channels
):
    length = query_matrix.shape[0]
    channel_log_decay = channel_log_decays(decay_logits, position_log_decay, key_channels)
    query_f = query_matrix.astype(jnp.float32).reshape(length, -1, key_channels)
    key_f = key_matrix.astype(jnp.float32).reshape(length, -1, key_channels)
    value_f = value_matrix.astype(jnp.float32).reshape(length, -1, DV)
    return (query_f, key_f, value_f, channel_log_decay)


def flipped(members):
    return tuple((jnp.flip(member, axis=0) for member in members))


def end_state(members):
    key_f, value_f, channel_log_decay = (members[1], members[2], members[3])
    totals = jnp.sum(channel_log_decay, axis=0)
    running = jnp.cumsum(channel_log_decay, axis=0)
    weighted = key_f * jnp.exp(totals[None] - running)
    states = jnp.einsum("thd,thv->hdv", weighted, value_f)
    return (totals, states)


def chain_combine(earlier, later):
    joined = []
    for member in range(0, len(earlier), 2):
        joined.append(earlier[member] + later[member])
        joined.append(earlier[member + 1] * jnp.exp(later[member])[..., None] + later[member + 1])
    return tuple(joined)


def finish(forward, backward, gate_values, per_head_norm_gain):
    both = forward + backward
    scale = lax.rsqrt(jnp.mean(both * both, axis=-1, keepdims=True) + norm_eps)
    gated = (
        both
        * scale
        * per_head_norm_gain
        * jax.nn.silu(gate_values.astype(jnp.float32).reshape(both.shape))
    )
    return gated.reshape(both.shape[0], -1).astype(jnp.bfloat16)


def rms_rows(rows, feedforward_norm_gain):
    scale = lax.rsqrt(jnp.mean(rows * rows, axis=-1, keepdims=True) + norm_eps)
    return (rows * scale * feedforward_norm_gain).astype(jnp.bfloat16)


def per_device(
    stream,
    first_group_queries,
    first_group_keys,
    first_group_values,
    first_gate_logits,
    first_decay_logits,
    second_group_queries,
    second_group_keys,
    second_group_values,
    second_gate_logits,
    second_decay_logits,
    position_log_decay,
    per_head_norm_gain,
    first_output_weight,
    second_output_weight,
    feedforward_norm_gain,
    gate_weight,
    up_weight,
    down_weight,
):
    tok_rows = stream.shape[0]
    first_group = prepare_inputs(
        first_group_queries,
        first_group_keys,
        first_group_values,
        first_decay_logits,
        position_log_decay,
        KEY_SIZE_FIRST,
    )
    second_group = prepare_inputs(
        second_group_queries,
        second_group_keys,
        second_group_values,
        second_decay_logits,
        position_log_decay,
        KEY_SIZE_SECOND,
    )
    first_back = flipped(first_group)
    second_back = flipped(second_group)
    ahead_first = end_state(first_group)
    ahead_second = end_state(second_group)
    behind_first = end_state(first_back)
    behind_second = end_state(second_back)
    blank = (
        jnp.zeros_like(ahead_first[0]),
        jnp.zeros_like(ahead_first[1]),
        jnp.zeros_like(ahead_second[0]),
        jnp.zeros_like(ahead_second[1]),
    )
    forward_in = carried_in(
        (ahead_first[0], ahead_first[1], ahead_second[0], ahead_second[1]),
        SP,
        chain_combine,
        blank,
        False,
    )
    backward_in = carried_in(
        (behind_first[0], behind_first[1], behind_second[0], behind_second[1]),
        SP,
        chain_combine,
        blank,
        True,
    )
    carried = (forward_in[1], backward_in[1], forward_in[3], backward_in[3])
    forward_first = one_way(
        first_group[0], first_group[1], first_group[2], first_group[3], carried[0]
    )
    backward_first = jnp.flip(
        one_way(first_back[0], first_back[1], first_back[2], first_back[3], carried[1]), 0
    )
    forward_second = one_way(
        second_group[0], second_group[1], second_group[2], second_group[3], carried[2]
    )
    backward_second = jnp.flip(
        one_way(second_back[0], second_back[1], second_back[2], second_back[3], carried[3]), 0
    )
    first_group_output = finish(
        forward_first, backward_first, first_gate_logits, per_head_norm_gain
    )
    second_group_output = finish(
        forward_second, backward_second, second_gate_logits, per_head_norm_gain
    )
    part_rows = tok_rows // lax.axis_size("tp")
    row_start = lax.axis_index("tp") * part_rows
    summed = summed_on_arrival(
        (
            jnp.dot(first_group_output, first_output_weight, preferred_element_type=jnp.float32)
            + jnp.dot(second_group_output, second_output_weight, preferred_element_type=jnp.float32)
        ).astype(jnp.bfloat16),
        "tp",
        0,
    )
    own_residual = (
        lax.dynamic_slice_in_dim(stream, row_start, part_rows, 0).astype(jnp.float32) + summed
    )
    normed_all = collect(rms_rows(own_residual, feedforward_norm_gain), "tp", 0)
    pieces = side_by_side((gate_weight, up_weight), SP, 0, 1)
    gate_sum = jnp.dot(normed_all, pieces[0], preferred_element_type=jnp.float32)
    up_sum = jnp.dot(normed_all, pieces[1], preferred_element_type=jnp.float32)
    hidden = (jax.nn.silu(gate_sum) * up_sum).astype(jnp.bfloat16)
    down_whole = gather_axes(down_weight, SP, 1)
    down_sum = summed_on_arrival(
        jnp.dot(hidden, down_whole, preferred_element_type=jnp.float32).astype(jnp.bfloat16),
        "tp",
        0,
    )
    return (own_residual + 0.5 * down_sum).astype(jnp.bfloat16)


def solution(mesh):
    split = Mesh(mesh.devices.reshape(8, 4, mesh.shape["tp"]), ("sp_0", "sp_1", "tp"))
    placed = (
        P(SP, None),
        P(SP, "tp"),
        P(SP, "tp"),
        P(SP, "tp"),
        P(SP, "tp"),
        P(SP, "tp"),
        P(SP, "tp"),
        P(SP, "tp"),
        P(SP, "tp"),
        P(SP, "tp"),
        P(SP, "tp"),
        P(SP),
        P(),
        P("tp", None),
        P("tp", None),
        P(),
        P(SP, "tp"),
        P(SP, "tp"),
        P("tp", SP),
    )
    return jax.shard_map(
        per_device, mesh=split, in_specs=placed, out_specs=P(SP_TP, None), check_vma=False
    )
```

profile of v0, /device:TPU:1, one launch (start us, length us, event | category | flops | bytes accessed | tf_op | source)
XLA Modules:
  0.0 234.1 jit_solution(4798904906511506640)
XLA Ops:
  6.6 1.8 pad_maximum_fusion
  8.4 13.0 %all_gather.42 = bf16[704,256]{0,1:T(8,128)(2,1)} all-gather(bf16[704,64]{0,1:T(8,128)(2,1)} %param.45), channel_id=1, replica_groups=mesh['sp_0'=8,'sp_1'=4,'tp'=8] {'sp_1'}, dimensions={1}, use_global_device_ids=true | all-gather | bytes 450560 | tf_op jit(solution)/shard_map/all_gather | solution.py:104
  21.5 1.0 fusion.222
  22.6 0.9 fusion.216
  27.9 9.5 %all-gather.4 = bf16[4,194,128]{2,1,0:T(8,128)(2,1)S(1)} all-gather(bf16[1,194,128]{2,1,0:T(8,128)(2,1)S(1)} %maximum_bitcast_fusion), channel_id=2, replica_groups=mesh['sp_0'=8,'sp_1'=4,'tp'=8] {'sp_1'}, dimensions={0}, use_global_device_ids=true | all-gather | bytes 248320 | tf_op jit(solution)/shard_map/all_gather | solution.py:33
  39.2 23.6 %all-gather.5 = bf16[8,194,128]{2,1,0:T(8,128)(2,1)S(1)} all-gather(bf16[1,194,128]{2,1,0:T(8,128)(2,1)S(1)} %maximum_bitcast_fusion.1), channel_id=3, replica_groups=mesh['sp_0'=8,'sp_1'=4,'tp'=8] {'sp_0'}, dimensions={0}, use_global_device_ids=true | all-gather | bytes 446976 | tf_op jit(solution)/shard_map/all_gather | solution.py:33
  63.4 0.8 copy.185
  65.3 11.7 %all-gather.6 = bf16[4,194,128]{2,1,0:T(8,128)(2,1)S(1)} all-gather(bf16[1,194,128]{2,1,0:T(8,128)(2,1)S(1)} %maximum_bitcast_fusion.2), channel_id=4, replica_groups=mesh['sp_0'=8,'sp_1'=4,'tp'=8] {'sp_1'}, dimensions={0}, use_global_device_ids=true | all-gather | bytes 248320 | tf_op jit(solution)/shard_map/all_gather | solution.py:33
  78.4 22.6 %all-gather.7 = bf16[8,194,128]{2,1,0:T(8,128)(2,1)S(1)} all-gather(bf16[1,194,128]{2,1,0:T(8,128)(2,1)S(1)} %maximum_bitcast_fusion.3), channel_id=5, replica_groups=mesh['sp_0'=8,'sp_1'=4,'tp'=8] {'sp_0'}, dimensions={0}, use_global_device_ids=true | all-gather | bytes 446976 | tf_op jit(solution)/shard_map/all_gather | solution.py:33
  102.5 0.8 reverse.24
  103.6 1.0 select_add_fusion.1
  105.2 3.9 %while.50 = (s32[]{:T(128)}, f32[1,128,128]{2,1,0:T(8,128)S(1)}, f32[4,1,64,128]{3,2,1,0:T(8,128)}, f32[4,1,1,128]{3,2,1,0:T(1,128)S(1)}, bf16[4,1,64,128]{3,2,1...) while((s32[]{:T(128)}, f32[1,128,128]{2,1,0:T(8,128)S(1)}, ...), condition=%wide.region_21.22_spmd, body=%wide.region_20.21_spmd.sunk | while | flops 4227074 | bytes 282201 | solution.py:145
  106.2 0.7 fusion.302
  107.2 0.7 fusion.302
  108.1 0.7 fusion.302
  109.3 1.0 select_add_fusion
  111.0 3.9 %while.51 = (s32[]{:T(128)}, f32[1,128,128]{2,1,0:T(8,128)S(1)}, f32[4,1,64,128]{3,2,1,0:T(8,128)}, f32[4,1,1,128]{3,2,1,0:T(1,128)S(1)}, bf16[4,1,64,128]{3,2,1...) while((s32[]{:T(128)}, f32[1,128,128]{2,1,0:T(8,128)S(1)}, ...), condition=%wide.region_24.25_spmd, body=%wide.region_23.24_spmd.sunk | while | flops 4227074 | bytes 282201 | solution.py:145
  111.9 0.7 fusion.309
  112.9 0.7 fusion.309
  113.9 0.7 fusion.309
  115.5 1.0 reduce_window_sum.104
  117.2 0.9 select_add_fusion.3
  118.1 6.8 %while.48 = (s32[]{:T(128)}, f32[1,64,128]{2,1,0:T(8,128)S(1)}, f32[4,1,64,128]{3,2,1,0:T(8,128)S(1)}, f32[4,1,1,64]{3,2,1,0:T(1,128)}, bf16[4,1,64,64]{3,2,1,0:...) while((s32[]{:T(128)}, f32[1,64,128]{2,1,0:T(8,128)S(1)}, ...), condition=%wide.region_8.9_spmd, body=%wide.region_7.8_spmd.sunk | while | flops 2113538 | bytes 183385 | solution.py:145
  118.2 0.9 fusion.288
  119.9 0.8 fusion.288
  121.6 0.8 fusion.288
  123.3 0.8 fusion.288
  125.9 1.0 copy.168
  127.6 0.9 select_add_fusion.2
  128.5 4.2 %while.49 = (s32[]{:T(128)}, f32[1,64,128]{2,1,0:T(8,128)S(1)}, f32[4,1,64,128]{3,2,1,0:T(8,128)S(1)}, f32[4,1,1,64]{3,2,1,0:T(1,128)S(1)}, bf16[4,1,64,64]{3,2,...) while((s32[]{:T(128)}, f32[1,64,128]{2,1,0:T(8,128)S(1)}, ...), condition=%wide.region_17.18_spmd, body=%wide.region_16.17_spmd.sunk | while | flops 2113538 | bytes 183385 | solution.py:145
  128.5 0.9 fusion.295
  129.6 0.8 fusion.295
  130.6 0.8 fusion.295
  131.6 0.8 fusion.295
  132.7 1.0 fusion.64
  133.7 1.0 fusion.66
  134.7 1.0 fusion.65
  136.5 1.3 fusion.129
  137.9 1.5 fusion.56
  139.4 20.5 %all-to-all-start = ((bf16[8,32,2048]{2,1,0:T(8,128)(2,1)}), bf16[8,32,2048]{2,1,0:T(8,128)(2,1)S(1)}, u32[]{:S(2)}, u32[]{:S(2)}) async-start(bf16[8,32,2048]{2,1,0:T(8,128)(2,1)} %bitcast.191), calls=%async_computation | async-start | bytes 2097152 | tf_op jit(solution)/shard_map/all_to_all | solution.py:73
  159.9 15.0 %all-to-all-done = bf16[8,32,2048]{2,1,0:T(8,128)(2,1)S(1)} async-done(((bf16[8,32,2048]{2,1,0:T(8,128)(2,1)}), bf16[8,32,2048]{2,1,0:T(8,128)(2,1)S(1)}, u32[]{:S(2)}, u32[]{:S(2)}) %all-to-all-start) | async-done | bytes 1048608 | tf_op jit(solution)/shard_map/all_to_all | solution.py:73
  175.0 1.1 multiply_reduce_fusion
  176.1 1.0 multiply_convert_fusion
  177.2 18.3 %all_to_all.15 = bf16[8,32,2048]{2,1,0:T(8,128)(2,1)S(1)} all-to-all(bf16[8,32,2048]{2,1,0:T(8,128)(2,1)S(1)} %broadcast_in_dim.46), channel_id=1, replica_groups=mesh['sp_0'=8,'sp_1'=4,'tp'=8] {'tp'}, dimensions={0} | all-to-all | bytes 2097152 | tf_op jit(solution)/shard_map/all_to_all | solution.py:79
  195.6 4.1 %fusion.54 = f32[256,704]{0,1:T(8,128)} fusion(bf16[256,2048]{1,0:T(8,128)(2,1)S(1)} %bitcast.616, bf16[2048,1408]{1,0:T(8,128)(2,1)} %all-gather.11.cloned.1.call-done), kind=kOutput, calls=%fused_computation.66 | convolution fusion | flops 738197504 | bytes 4915200 | tf_op jit(solution)/shard_map/dot_general | solution.py:296
  199.7 7.4 %convolution_convert_fusion = bf16[256,2048]{1,0:T(8,128)(2,1)S(1)} fusion(bf16[704,2048]{0,1:T(8,128)(2,1)} %all-gather.13.cloned.1.call-done, bf16[256,2048]{1,0:T(8,128)(2,1)S(1)} %bitcast.617, bf16[2048,1408]{1,0:T(8,128)(2,1)} %all-gather.11.cloned.1.call-done, f32[256,704]{0,1:T(8,128)} %fusion.54), kind=kOutput, calls=%fused_computation.70 | convolution fusion | flops 1478000640 | bytes 9109504 | tf_op jit(solution)/shard_map/dot_general | solution.py:301
  207.1 18.4 %all_to_all.16 = bf16[8,32,2048]{2,1,0:T(8,128)(2,1)S(1)} all-to-all(bf16[8,32,2048]{2,1,0:T(8,128)(2,1)S(1)} %bitcast.618), channel_id=1, replica_groups=mesh['sp_0'=8,'sp_1'=4,'tp'=8] {'tp'}, dimensions={0} | all-to-all | bytes 2097152 | tf_op jit(solution)/shard_map/all_to_all | solution.py:73
  225.6 1.6 add_convert_fusion
  (207 shorter events, 23.8 us)
Async XLA Ops:
  6.5 130.0 %copy-start = (bf16[128,2048]{1,0:T(8,128)(2,1)S(1)}, bf16[128,2048]{1,0:T(8,128)(2,1)}, u32[]{:S(2)}) copy-start(bf16[128,2048]{1,0:T(8,128)(2,1)} %param.40) | copy-start | bytes 1572868
  6.5 18.7 %copy-start.3 = (bf16[256,128]{1,0:T(8,128)(2,1)S(1)}, bf16[256,128]{1,0:T(8,128)(2,1)}, u32[]{:S(2)}) copy-start(bf16[256,128]{1,0:T(8,128)(2,1)} %param.34) | copy-start | bytes 196612
  6.5 19.9 %copy-start.9 = (bf16[256,64]{0,1:T(8,128)(2,1)S(1)}, bf16[256,64]{0,1:T(8,128)(2,1)}, u32[]{:S(2)}) copy-start(bf16[256,64]{0,1:T(8,128)(2,1)} %param.29) | copy-start | bytes 98308
  6.5 20.1 %copy-start.10 = (bf16[256,128]{1,0:T(8,128)(2,1)S(1)}, bf16[256,128]{1,0:T(8,128)(2,1)}, u32[]{:S(2)}) copy-start(bf16[256,128]{1,0:T(8,128)(2,1)} %param.33) | copy-start | bytes 196612
  6.5 20.2 %copy-start.2 = (bf16[256,128]{1,0:T(8,128)(2,1)S(1)}, bf16[256,128]{1,0:T(8,128)(2,1)}, u32[]{:S(2)}) copy-start(bf16[256,128]{1,0:T(8,128)(2,1)} %param.35) | copy-start | bytes 196612
  6.5 20.8 %copy-start.1 = (bf16[256,128]{1,0:T(8,128)(2,1)S(1)}, bf16[256,128]{1,0:T(8,128)(2,1)}, u32[]{:S(2)}) copy-start(bf16[256,128]{1,0:T(8,128)(2,1)} %param.30) | copy-start | bytes 196612
  6.6 189.0 %all-gather.11.cloned.1.call-start = ((), (), s32[]{:S(2)}) async-start(), calls=%async_computation.3 | async-start | bytes 5947392 | tf_op jit(solution)/shard_map/all_gather | solution.py:98
  8.4 191.3 %all-gather.13.cloned.1.call-start = ((), (), s32[]{:S(2)}) async-start(), calls=%async_computation.4 | async-start | bytes 3538944 | tf_op jit(solution)/shard_map/all_gather | solution.py:104
  26.9 75.5 %copy-start.12 = (bf16[256,64]{0,1:T(8,128)(2,1)S(1)}, bf16[256,64]{0,1:T(8,128)(2,1)}, u32[]{:S(2)}) copy-start(bf16[256,64]{0,1:T(8,128)(2,1)} %param.28) | copy-start | bytes 98308
  38.6 0.6 copy-start.21
  38.6 0.6 copy-start.22
  38.6 0.6 copy-start.23
  38.6 26.7 %copy-start.20 = (f32[64]{0:T(128)}, f32[64]{0:T(128)S(1)}, u32[]{:S(2)}) copy-start(f32[64]{0:T(128)S(1)} %get-tuple-element.278) | copy-start | bytes 772
  77.6 25.7 %copy-start.24 = (f32[128]{0:T(128)}, f32[128]{0:T(128)S(1)}, u32[]{:S(2)}) copy-start(f32[128]{0:T(128)S(1)} %get-tuple-element.249) | copy-start | bytes 1540
  77.6 25.9 %copy-start.25 = (f32[128]{0:T(128)}, f32[128]{0:T(128)S(1)}, u32[]{:S(2)}) copy-start(f32[128]{0:T(128)S(1)} %get-tuple-element.250) | copy-start | bytes 1540
  78.1 25.3 %copy-start.16 = (f32[64]{0:T(128)}, f32[64]{0:T(128)S(1)}, u32[]{:S(2)}) copy-start(f32[64]{0:T(128)S(1)} %get-tuple-element.282) | copy-start | bytes 772
  78.1 25.3 %copy-start.17 = (f32[64]{0:T(128)}, f32[64]{0:T(128)S(1)}, u32[]{:S(2)}) copy-start(f32[64]{0:T(128)S(1)} %get-tuple-element.283) | copy-start | bytes 772
  78.1 25.4 %copy-start.18 = (f32[64]{0:T(128)}, f32[64]{0:T(128)S(1)}, u32[]{:S(2)}) copy-start(f32[64]{0:T(128)S(1)} %get-tuple-element.284) | copy-start | bytes 772
  78.1 25.4 %copy-start.19 = (f32[64]{0:T(128)}, f32[64]{0:T(128)S(1)}, u32[]{:S(2)}) copy-start(f32[64]{0:T(128)S(1)} %get-tuple-element.285) | copy-start | bytes 772
  116.5 0.7 copy-start.15
  118.1 14.6 %copy-start.5 = (f32[4,1,64,128]{3,2,1,0:T(8,128)S(1)}, f32[4,1,64,128]{3,2,1,0:T(8,128)}, u32[]{:S(2)}) copy-start(f32[4,1,64,128]{3,2,1,0:T(8,128)} %get-tuple-element.155) | copy-start | bytes 393220
  125.0 0.8 copy-start.7
  125.0 11.1 %copy-start.11 = (pred[64,64]{1,0:T(8,128)(4,1)S(1)}, pred[64,64]{1,0:T(8,128)(4,1)}, u32[]{:S(2)}) copy-start(pred[64,64]{1,0:T(8,128)(4,1)} %iota_compare_fusion) | copy-start | bytes 12292
  125.9 7.8 %copy-start.6 = (f32[4,1,64,128]{3,2,1,0:T(8,128)S(1)}, f32[4,1,64,128]{3,2,1,0:T(8,128)}, u32[]{:S(2)}) copy-start(f32[4,1,64,128]{3,2,1,0:T(8,128)} %get-tuple-element.156) | copy-start | bytes 393220
  127.6 9.0 %copy-start.26 = (f32[128]{0:T(128)S(1)}, f32[128]{0:T(128)}, u32[]{:S(2)}) copy-start(f32[128]{0:T(128)} %param.39) | copy-start | bytes 1540
  128.4 7.6 %copy-start.8 = (f32[4,1,64,128]{3,2,1,0:T(8,128)S(1)}, f32[4,1,64,128]{3,2,1,0:T(8,128)}, u32[]{:S(2)}) copy-start(f32[4,1,64,128]{3,2,1,0:T(8,128)} %copy-done.7) | copy-start | bytes 393220
  134.7 3.2 %copy-start.4 = (bf16[128,2048]{1,0:T(8,128)(2,1)S(1)}, bf16[128,2048]{1,0:T(8,128)(2,1)}, u32[]{:S(2)}) copy-start(bf16[128,2048]{1,0:T(8,128)(2,1)} %param.41) | copy-start | bytes 1572868
  134.7 3.2 %copy-start.13 = (bf16[256,128]{1,0:T(8,128)(2,1)S(1)}, bf16[256,128]{1,0:T(8,128)(2,1)}, u32[]{:S(2)}) copy-start(bf16[256,128]{1,0:T(8,128)(2,1)} %param.36) | copy-start | bytes 196612
  137.9 38.2 %copy-start.14 = (f32[2048]{0:T(1024)S(1)}, f32[2048]{0:T(1024)}, u32[]{:S(2)}) copy-start(f32[2048]{0:T(1024)} %param.42) | copy-start | bytes 24580
  139.4 35.5 %all-to-all-start = ((bf16[8,32,2048]{2,1,0:T(8,128)(2,1)}), bf16[8,32,2048]{2,1,0:T(8,128)(2,1)S(1)}, u32[]{:S(2)}, u32[]{:S(2)}) async-start(bf16[8,32,2048]{2,1,0:T(8,128)(2,1)} %bitcast.191), calls=%async_computation | async-start | bytes 2097152 | tf_op jit(solution)/shard_map/all_to_all | solution.py:73
Sparse Core Ops, SparseCore 0:
  9.9 91.4 all-gather.10
  103.2 42.6 all-gather.12
where the time goes:
time: 235 us; the launch traced here: 234 us
  blocking collectives  117 us (50%)
  matrix products  34.2 us (15%)
  other arithmetic  22 us (9%)
  starting transfers between devices  20.6 us (9%)
  waiting for transfers between devices  15 us (6%)
  between operations  14.2 us (6%)
  local copies, waits for them, and re-layouts  10.8 us (5%)
    all_gather x4, blocking collectives, gathered_once(): both, at, found = (lax.all_gather(jnp.concatenate(lines), axis), 0, {})  67.3 us
    all_to_all x1, starting transfers between devices, summed_on_arrival(): blocks = lax.all_to_all(cut_along(value, dim, size), axis, 0, 0, tiled=True)  20.5 us
    all_to_all x1, blocking collectives, summed_on_arrival(): blocks = lax.all_to_all(cut_along(value, dim, size), axis, 0, 0, tiled=True)  18.4 us
    all_to_all x1, blocking collectives, copy_for_each(): lax.all_to_all(jnp.broadcast_to(value[None], (size, *value.shape)), axis,...  18.3 us
    all_to_all x1, waiting for transfers between devices, summed_on_arrival(): blocks = lax.all_to_all(cut_along(value, dim, size), axis, 0, 0, tiled=True)  15 us
    all_gather x1, blocking collectives, gather_axes(): value = lax.all_gather(value, axis, axis=dim, tiled=True)  13 us
    dot_general x16, matrix products, advance(): emitted = jnp.einsum('hid,hdv->hiv', query_part, states)  12.7 us
    dot_general x1, matrix products, per_device(): jnp.dot(hidden, down_whole, preferred_element_type=jnp.float32)  7.39 us
  transfers between devices with their start and end apart: 3, of which 1 were waited for; matrix products, arithmetic and copies ran while one was open for 24% of the time, Pallas kernels for 0%

commit v1 on v0

v1 whole, which is shorter than its diff:
```python
import jax
import jax.numpy as jnp
from jax import lax
from jax.experimental import pallas as pl
from jax.experimental.pallas import tpu as pltpu
from jax.sharding import Mesh
from jax.sharding import PartitionSpec as P

DV = 128
SP = ("z", "y")
TP = ("x", "c")
SIZES = {"z": 8, "y": 4, "x": 4, "c": 2}
HIGH = lax.Precision.HIGHEST
F32 = jnp.float32
BF16 = jnp.bfloat16

decay_softness = 16.0
norm_eps = 1e-06


def shift(value, axis, by):
    n = SIZES[axis]
    return lax.ppermute(value, axis, [(i, (i + by) % n) for i in range(n)])


def log_decays(decay_ref):
    d = decay_ref[...].astype(F32)
    return (jnp.minimum(d, 0.0) - jnp.log1p(jnp.exp(-jnp.abs(d)))) / decay_softness


def lower_mask(n):
    return lax.broadcasted_iota(jnp.int32, (n, n), 0) >= lax.broadcasted_iota(jnp.int32, (n, n), 1)


def position_sums(pos_ref):
    n = pos_ref.shape[1]
    rows = jnp.broadcast_to(pos_ref[...], (n, n))
    low = lower_mask(n)
    diag = lax.broadcasted_iota(jnp.int32, (n, n), 0) == lax.broadcasted_iota(jnp.int32, (n, n), 1)
    upto = jnp.sum(jnp.where(low, rows, 0.0), axis=1, keepdims=True)
    before = jnp.sum(jnp.where(low & ~diag, rows, 0.0), axis=1, keepdims=True)
    return upto, before


def running_sums(logd, upto, before):
    n = logd.shape[0]
    tri = jnp.where(lower_mask(n), 1.0, 0.0).astype(F32)
    cum = jnp.dot(tri, logd, precision=HIGH, preferred_element_type=F32)
    return cum + upto, (cum - logd) + before


def rows_contracted(a, b, precision=None):
    return lax.dot_general(
        a, b, (((0,), (0,)), ((), ())), precision=precision, preferred_element_type=F32
    )


def lanes_contracted(a, b):
    return lax.dot_general(a, b, (((1,), (1,)), ((), ())), preferred_element_type=F32)


def states_kernel(ka, va, da, kb, vb, db, pos, msg):
    upto, before = position_sums(pos)
    n = pos.shape[1]
    pos_total = jnp.sum(pos[...], axis=1, keepdims=True)
    ones = jnp.ones((n, DV), F32)
    at = 0
    for k_ref, v_ref, d_ref in ((kb, vb, db), (ka, va, da)):
        logd = log_decays(d_ref)
        upto_l, before_l = running_sums(logd, upto, before)
        total = upto_l[n - 1 : n, :]
        key = k_ref[...].astype(F32)
        value = v_ref[...]
        ahead = rows_contracted((key * jnp.exp(total - upto_l)).astype(BF16), value)
        behind = rows_contracted((key * jnp.exp(before_l)).astype(BF16), value)
        totals = rows_contracted(logd, ones, HIGH) + pos_total
        high = totals.astype(BF16).astype(F32)
        lane = lax.broadcasted_iota(jnp.int32, totals.shape, 1)
        both = jnp.where(lane < 64, high, totals - high)
        groups = logd.shape[1] // 8
        part = jnp.concatenate(
            [x.reshape(groups, 8, DV) for x in (ahead, behind, both)], axis=1
        )
        msg[at : at + groups] = part.astype(BF16)
        at += groups
    msg[at:] = jnp.zeros((msg.shape[0] - at, *msg.shape[1:]), BF16)


def scan_kernel(msg, out):
    n = msg.shape[0]
    blocks = msg[...].astype(F32)
    decay = jnp.exp(blocks[:, 16:24, 0:1] + blocks[:, 16:24, 64:65])
    run = jnp.zeros((8, DV), F32)
    ahead = []
    for k in range(n):
        ahead.append(run)
        run = run * decay[k] + blocks[k, 0:8, :]
    run = jnp.zeros((8, DV), F32)
    behind = []
    for k in reversed(range(n)):
        behind.append(run)
        run = run * decay[k] + blocks[k, 8:16, :]
    behind.reverse()
    for k in range(n):
        out[k] = jnp.concatenate([ahead[k], behind[k]], axis=0).astype(BF16)


def local_kernel(qa, ka, va, da, qb, kb, vb, db, pos, out, qf_out, qb_out):
    n = pos.shape[1]
    half = n // 2
    upto, before = position_sums(pos)
    low = lower_mask(half)
    up = lax.broadcasted_iota(jnp.int32, (half, half), 0) <= lax.broadcasted_iota(
        jnp.int32, (half, half), 1
    )
    for g, (q_ref, k_ref, v_ref, d_ref) in enumerate(((qa, ka, va, da), (qb, kb, vb, db))):
        inc, exc = running_sums(log_decays(d_ref), upto, before)
        q = q_ref[...].astype(F32)
        k = k_ref[...].astype(F32)
        total = inc[n - 1 : n, :]
        lo = 0 if g == 1 else 128
        width = q.shape[1]
        qf_out[:, lo : lo + width] = (q * jnp.exp(inc)).astype(BF16)
        qb_out[:, lo : lo + width] = (q * jnp.exp(total - exc)).astype(BF16)
        diag = []
        for b in range(2):
            s = slice(b * half, (b + 1) * half)
            m = inc[b * half + half // 2 - 1 : b * half + half // 2, :]
            ahead = lanes_contracted(
                (q[s] * jnp.exp(inc[s] - m)).astype(BF16), (k[s] * jnp.exp(m - inc[s])).astype(BF16)
            )
            behind = lanes_contracted(
                (q[s] * jnp.exp(m - exc[s])).astype(BF16), (k[s] * jnp.exp(exc[s] - m)).astype(BF16)
            )
            diag.append(jnp.where(low, ahead, 0.0) + jnp.where(up, behind, 0.0))
        m = inc[half - 1 : half, :]
        first, second = slice(0, half), slice(half, n)
        down = lanes_contracted(
            (q[second] * jnp.exp(inc[second] - m)).astype(BF16),
            (k[first] * jnp.exp(m - inc[first])).astype(BF16),
        )
        upper = lanes_contracted(
            (q[first] * jnp.exp(m - exc[first])).astype(BF16),
            (k[second] * jnp.exp(exc[second] - m)).astype(BF16),
        )
        weights = jnp.concatenate(
            [
                jnp.concatenate([diag[0], upper], axis=1),
                jnp.concatenate([down, diag[1]], axis=1),
            ],
            axis=0,
        ).astype(BF16)
        out[:, g * DV : (g + 1) * DV] = jnp.dot(weights, v_ref[...], preferred_element_type=F32)


def finish_kernel(local, qf, qb, states, ga, gb, gain, out):
    groups = states[...].astype(F32)[:24]
    ahead = groups[:, 0:8, :].reshape(192, DV).astype(BF16)
    behind = groups[:, 8:16, :].reshape(192, DV).astype(BF16)
    for g, gate_ref in enumerate((ga, gb)):
        lo, hi = (0, 128) if g == 1 else (128, 192)
        both = (
            local[:, g * DV : (g + 1) * DV]
            + jnp.dot(qf[:, lo:hi], ahead[lo:hi], preferred_element_type=F32)
            + jnp.dot(qb[:, lo:hi], behind[lo:hi], preferred_element_type=F32)
        )
        scale = lax.rsqrt(jnp.mean(both * both, axis=-1, keepdims=True) + norm_eps)
        gate = gate_ref[...].astype(F32)
        silu = gate / (1.0 + jnp.exp(-gate))
        out[:, g * DV : (g + 1) * DV] = (both * scale * gain[...] * silu).astype(BF16)


def call(kernel, out_shape, flops, *args):
    return pl.pallas_call(
        kernel,
        out_shape=out_shape,
        cost_estimate=pl.CostEstimate(flops=flops, bytes_accessed=10**6, transcendentals=10**5),
    )(*args)


def around_x(value):
    rows = value.shape[0] // 2
    left, right = shift(value, "x", 1), shift(value, "x", -1)
    far_top = shift(left[:rows], "x", 1)
    far_low = shift(right[rows:], "x", -1)
    return jnp.concatenate([value, left, right, far_top, far_low], axis=0)


def per_device(
    stream,
    first_group_queries,
    first_group_keys,
    first_group_values,
    first_gate_logits,
    first_decay_logits,
    second_group_queries,
    second_group_keys,
    second_group_values,
    second_gate_logits,
    second_decay_logits,
    position_log_decay,
    per_head_norm_gain,
    first_output_weight,
    second_output_weight,
    feedforward_norm_gain,
    gate_weight,
    up_weight,
    down_weight,
):
    tokens, width = stream.shape
    chips = SIZES["x"]
    part = tokens // (chips * 2)
    core = lax.axis_index("c")
    place = lax.axis_index("x")

    gate_up = lax.all_gather(
        jnp.concatenate([gate_weight, up_weight], axis=1), SP, axis=0, tiled=True
    )
    down_whole = lax.all_gather(down_weight, SP, axis=1, tiled=True)

    pos = position_log_decay.reshape(1, tokens)
    messages = call(
        states_kernel,
        jax.ShapeDtypeStruct((32, 24, DV), BF16),
        10**8,
        first_group_keys,
        first_group_values,
        first_decay_logits,
        second_group_keys,
        second_group_values,
        second_decay_logits,
        pos,
    )
    arrived = lax.all_to_all(messages, SP, 0, 0, tiled=True)

    out_own = jnp.concatenate([first_output_weight, second_output_weight], axis=0)
    out_same = around_x(out_own)
    out_other = shift(out_same, "c", 1)

    local, query_ahead, query_behind = call(
        local_kernel,
        (
            jax.ShapeDtypeStruct((tokens, 2 * DV), F32),
            jax.ShapeDtypeStruct((tokens, 192), BF16),
            jax.ShapeDtypeStruct((tokens, 192), BF16),
        ),
        2 * 10**8,
        first_group_queries,
        first_group_keys,
        first_group_values,
        first_decay_logits,
        second_group_queries,
        second_group_keys,
        second_group_values,
        second_decay_logits,
        pos,
    )
    scanned = call(scan_kernel, jax.ShapeDtypeStruct((32, 16, DV), BF16), 10**7, arrived)
    states = lax.all_to_all(scanned, SP, 0, 0, tiled=True)
    mixed = call(
        finish_kernel,
        jax.ShapeDtypeStruct((tokens, 2 * DV), BF16),
        10**8,
        local,
        query_ahead,
        query_behind,
        states,
        first_gate_logits,
        second_gate_logits,
        per_head_norm_gain.reshape(1, DV),
    )
    left, right, far = shift(mixed, "x", 1), shift(mixed, "x", -1), shift(mixed, "x", 2)
    mixed_same = jnp.concatenate([mixed, left, right, far], axis=1)
    mixed_other = shift(mixed_same, "c", 1)
    residual = (
        stream.astype(F32)
        + jnp.dot(mixed_same, out_same, preferred_element_type=F32)
        + jnp.dot(mixed_other, out_other, preferred_element_type=F32)
    )
    scale = lax.rsqrt(jnp.mean(residual * residual, axis=-1, keepdims=True) + norm_eps)
    normed = (residual * scale * feedforward_norm_gain).astype(BF16)
    sums = jnp.dot(normed, gate_up, preferred_element_type=F32)
    units = gate_weight.shape[1]
    hidden = (jax.nn.silu(sums[:, :units]) * sums[:, units:]).astype(BF16)

    by_core = hidden.reshape(chips, 2, part, units)

    def partial_sums(which):
        rows = lax.dynamic_index_in_dim(by_core, which, 1, keepdims=False).reshape(-1, units)
        return jnp.dot(rows, down_whole, preferred_element_type=F32).astype(BF16)

    theirs = shift(partial_sums(1 - core), "c", 1)
    pair = (partial_sums(core).astype(F32) + theirs.astype(F32)).astype(BF16)
    blocks = lax.all_to_all(pair.reshape(chips, part, width), "x", 0, 0, tiled=True)
    down_sum = jnp.sum(blocks.astype(F32), axis=0)
    own = lax.dynamic_slice_in_dim(residual, (place * 2 + core) * part, part, 0)
    return (own + 0.5 * down_sum).astype(BF16)


def solution(mesh):
    split = Mesh(mesh.devices.reshape(8, 4, 4, 2), ("z", "y", "x", "c"))
    placed = (
        P(SP, None),
        *(P(SP, TP),) * 10,
        P(SP),
        P(),
        P(TP, None),
        P(TP, None),
        P(),
        P(SP, TP),
        P(SP, TP),
        P(TP, SP),
    )
    return jax.shard_map(
        per_device, mesh=split, in_specs=placed, out_specs=P(SP + TP, None), check_vma=False
    )
```

time: 235 us -> 213 us (0.906)
  blocking collectives: 117 us -> 25.2 us
  waiting for transfers between devices: 15 us -> 99.7 us
  other arithmetic: 22 us -> 3.76 us
  matrix products: 34.2 us -> 17.1 us
  Pallas kernels: 0 us -> 11.2 us
  starting transfers between devices: 20.6 us -> 31 us
    all_gather x5 -> x0, blocking collectives: 80.3 us -> none  [the longest x4 67.3 us: gathered_once(): both, at, found = (lax.all_gather(jnp.concatenate(lines), axis), 0, {})]
    all_gather x2, waiting for transfers between devices: 0.01 us -> 48.4 us  [the longest x1 48.4 us: per_device(): down_whole = lax.all_gather(down_weight, SP, axis=1, tiled=True)]
    ppermute x0 -> x10, waiting for transfers between devices: none -> 36.1 us  [shift(): return lax.ppermute(value, axis, [(i, (i + by) % n) for i in range(n)])]
    ppermute x0 -> x10, starting transfers between devices: none -> 23 us  [shift(): return lax.ppermute(value, axis, [(i, (i + by) % n) for i in range(n)])]
    dot_general x44 -> x5, matrix products: 34.2 us -> 17.1 us  [the longest x2 5.14 us: partial_sums(): return jnp.dot(rows, down_whole, preferred_element_type=F32).astype(BF16)]
    all_to_all x1 -> x2, starting transfers between devices: 20.5 us -> 7.92 us  [the longest x1 3.97 us: per_device(): lax.all_to_all(pair.reshape(chips, part, width), 'x', 0, 0, tiled=True)]
    all_to_all x2 -> x1, blocking collectives: 36.7 us -> 25.2 us  [per_device(): arrived = lax.all_to_all(messages, SP, 0, 0, tiled=True)]
    pallas_call x0 -> x4, Pallas kernels: none -> 11.2 us  [call(): pl.pallas_call(kernel, out_shape=out_shape, cost_estimate=pl.CostEstimate...]
  transfers between devices with their start and end apart: 3 -> 14, of which waited for: 1 -> 10; matrix products, arithmetic and copies ran while one was open for 24% -> 11% of each run, Pallas kernels for 0% -> 5%
where the time goes in v1:
time: 213 us; the launch traced here: 212 us
  waiting for transfers between devices  99.7 us (47%)
  starting transfers between devices  31 us (15%)
  blocking collectives  25.2 us (12%)
  matrix products  17.1 us (8%)
  between operations  13.5 us (6%)
  Pallas kernels  11.2 us (5%)
  local copies, waits for them, and re-layouts  10.7 us (5%)
  other arithmetic  3.76 us (2%)
    all_gather x1, waiting for transfers between devices, per_device(): down_whole = lax.all_gather(down_weight, SP, axis=1, tiled=True)  48.4 us
    ppermute x10, waiting for transfers between devices, shift(): return lax.ppermute(value, axis, [(i, (i + by) % n) for i in range(n)])  36.1 us
    all_to_all x1, blocking collectives, per_device(): arrived = lax.all_to_all(messages, SP, 0, 0, tiled=True)  25.2 us
    ppermute x10, starting transfers between devices, shift(): return lax.ppermute(value, axis, [(i, (i + by) % n) for i in range(n)])  23 us
    pallas_call x4, Pallas kernels, call(): pl.pallas_call(kernel, out_shape=out_shape, cost_estimate=pl.CostEstimate...  11.2 us
    all_to_all x1, waiting for transfers between devices, per_device(): lax.all_to_all(pair.reshape(chips, part, width), 'x', 0, 0, tiled=True)  8.92 us
    unnamed x21, local copies, waits for them, and re-layouts  7.8 us
    all_to_all x1, waiting for transfers between devices, per_device(): states = lax.all_to_all(scanned, SP, 0, 0, tiled=True)  6.27 us
  transfers between devices with their start and end apart: 14, of which 10 were waited for; matrix products, arithmetic and copies ran while one was open for 11% of the time, Pallas kernels for 5%

profile of v1, /device:TPU:1, one launch (start us, length us, event | category | flops | bytes accessed | tf_op | source)
XLA Modules:
  0.0 212.2 jit_solution(9489798148417875691)
XLA Ops:
  6.5 1.7 pad_maximum_fusion.1
  8.3 0.0 all-gather.5.cloned.1.call-start
  8.3 2.0 constant_dynamic-update-slice_fusion.1
  10.3 2.0 constant_dynamic-update-slice_fusion
  12.3 2.0 collective-permute-start.3
  14.4 1.3 collective-permute-start.4
  15.7 20.7 %collective-permute-done.3 = bf16[256,2048]{1,0:T(8,128)(2,1)S(1)} collective-permute-done((bf16[256,2048]{1,0:T(8,128)(2,1)S(1)}, bf16[256,2048]{1,0:T(8,128)(2,1)S(1)}, u32[]{:S(2)}, u32[]{:S(2)}) %collective-permute-start.3) | collective-permute-done | bytes 1048608 | tf_op jit(solution)/shard_map/ppermute | solution.py:23
  36.5 1.9 collective-permute-start.5
  38.4 1.6 collective-permute-start.6
  40.0 1.0 constant_dynamic-update-slice_fusion.5
  41.0 1.1 constant_dynamic-update-slice_fusion.4
  42.1 7.0 %collective-permute-done.5 = bf16[128,2048]{1,0:T(8,128)(2,1)S(1)} collective-permute-done((bf16[128,2048]{1,0:T(8,128)(2,1)S(1)}, bf16[128,2048]{1,0:T(8,128)(2,1)S(1)}, u32[]{:S(2)}, u32[]{:S(2)}) %collective-permute-start.5) | collective-permute-done | bytes 524320 | tf_op jit(solution)/shard_map/ppermute | solution.py:23
  49.1 0.8 constant_dynamic-update-slice_fusion.3
  49.9 0.1 collective-permute-done.6
  50.0 0.8 constant_dynamic-update-slice_fusion.2
  50.8 3.5 %collective-permute-start.8 = (bf16[1024,2048]{1,0:T(8,128)(2,1)}, bf16[1024,2048]{1,0:T(8,128)(2,1)}, u32[]{:S(2)}, u32[]{:S(2)}) collective-permute-start(bf16[1024,2048]{1,0:T(8,128)(2,1)} %constant_dynamic-update-slice_fusion.2), channel_id=1, source_target_pairs={{0,1},{1,0},{2,3},{3,2},{4,5},{5,4},{6,7},{7,6},{8,9},{9,8},{10,11... | collective-permute-start | bytes 12582920 | tf_op jit(solution)/shard_map/ppermute | solution.py:23
  54.4 0.7 copy.21.ka
  55.1 0.7 copy.22.da
  55.8 3.4 %shard_map.182 = bf16[32,24,128]{2,1,0:T(8,128)(2,1)} custom-call(bf16[256,64]{1,0:T(8,128)(2,1)} %copy.21.ka, bf16[256,128]{1,0:T(8,128)(2,1)} %va.3, bf16[256,64]{1,0:T(8,128)(2,1)} %copy.22.da, bf16[256,128]{1,0:T(8,128)(2,1)} %kb.3, bf16[256,128]{1,0:T(8,128)(2,1)} %vb.3, bf16[256,128]{1,0:T(8,128)(2,1)} %db.3, f32[1,256]{1,0:T(1,128)} %bitcast.17), custom_call_target="tpu_custom_call" | custom-call | flops 100000000 | bytes 1000000 | tf_op jit(solution)/shard_map/pallas_call | solution.py:174
  59.3 25.2 %all_to_all.15.msg = bf16[32,24,128]{2,1,0:T(8,128)(2,1)} all-to-all(bf16[32,24,128]{2,1,0:T(8,128)(2,1)} %shard_map.182), channel_id=1, replica_groups=mesh['z'=8,'y'=4,'x'=4,'c'=2] {'z','y'}, dimensions={0} | all-to-all | bytes 393216 | tf_op jit(solution)/shard_map/all_to_all | solution.py:234
  84.4 1.8 shard_map.183
  86.2 4.0 %all-to-all-start.1 = ((bf16[32,16,128]{2,1,0:T(8,128)(2,1)}), bf16[32,16,128]{2,1,0:T(8,128)(2,1)S(1)}, u32[]{:S(2)}, u32[]{:S(2)}) async-start(bf16[32,16,128]{2,1,0:T(8,128)(2,1)} %shard_map.183), calls=%async_computation.1 | async-start | bytes 262144 | tf_op jit(solution)/shard_map/all_to_all | solution.py:259
  90.2 0.7 copy.20.qa
  90.9 3.9 %shard_map.181 = (f32[256,256]{1,0:T(8,128)}, bf16[256,192]{1,0:T(8,128)(2,1)}, bf16[256,192]{1,0:T(8,128)(2,1)}) custom-call(bf16[256,64]{1,0:T(8,128)(2,1)} %copy.20.qa, bf16[256,64]{1,0:T(8,128)(2,1)} %copy.21.ka, bf16[256,128]{1,0:T(8,128)(2,1)} %va.3, bf16[256,64]{1,0:T(8,128)(2,1)} %copy.22.da, bf16[256,128]{1,0:T(8,128)(2,1)} %qb.1, ...), custom_call_target="tpu_custom_call" | custom-call | flops 200000000 | bytes 1000000 | tf_op jit(solution)/shard_map/pallas_call | solution.py:174
  94.8 6.3 %all-to-all-done.1.states = bf16[32,16,128]{2,1,0:T(8,128)(2,1)S(1)} async-done(((bf16[32,16,128]{2,1,0:T(8,128)(2,1)}), bf16[32,16,128]{2,1,0:T(8,128)(2,1)S(1)}, u32[]{:S(2)}, u32[]{:S(2)}) %all-to-all-start.1) | async-done | bytes 131104 | tf_op jit(solution)/shard_map/all_to_all | solution.py:259
  101.1 0.6 copy-done.1
  101.7 2.1 %shard_map.184 = bf16[256,256]{1,0:T(8,128)(2,1)} custom-call(f32[256,256]{1,0:T(8,128)} %get-tuple-element.8.local, bf16[256,192]{1,0:T(8,128)(2,1)} %get-tuple-element.9.qf, bf16[256,192]{1,0:T(8,128)(2,1)} %get-tuple-element.10.qb, bf16[32,16,128]{2,1,0:T(8,128)(2,1)} %copy-done.1, bf16[256,128]{1,0:T(8,128)(2,1)} %ga.1, bf16[256,128]{1,0:T(8,128)(2,1)} %gb.1, ...), custom_call_target="tpu_custom_call" | custom-call | flops 100000000 | bytes 1000000 | tf_op jit(solution)/shard_map/pallas_call | solution.py:174
  103.8 2.7 %collective-permute-start.1 = (bf16[256,256]{1,0:T(8,128)(2,1)}, bf16[256,256]{1,0:T(8,128)(2,1)S(1)}, u32[]{:S(2)}, u32[]{:S(2)}) collective-permute-start(bf16[256,256]{1,0:T(8,128)(2,1)} %shard_map.184), channel_id=1, source_target_pairs={{0,6},{2,0},{4,2},{6,4},{1,7},{3,1},{5,3},{7,5},{8,14},{10,8},{12,... | collective-permute-start | bytes 393224 | tf_op jit(solution)/shard_map/ppermute | solution.py:23
  106.5 0.6 collective-permute-start.2
  107.1 2.0 collective-permute-done
  109.1 3.2 %collective-permute-done.2 = bf16[256,256]{1,0:T(8,128)(2,1)S(1)} collective-permute-done((bf16[256,256]{1,0:T(8,128)(2,1)}, bf16[256,256]{1,0:T(8,128)(2,1)S(1)}, u32[]{:S(2)}, u32[]{:S(2)}) %collective-permute-start.2) | collective-permute-done | bytes 131104 | tf_op jit(solution)/shard_map/ppermute | solution.py:23
  112.3 1.0 pad_maximum_fusion
  113.2 4.8 %collective-permute-start.7 = (bf16[256,1024]{1,0:T(8,128)(2,1)S(1)}, bf16[256,1024]{1,0:T(8,128)(2,1)S(1)}, u32[]{:S(2)}, u32[]{:S(2)}) collective-permute-start(bf16[256,1024]{1,0:T(8,128)(2,1)S(1)} %pad_maximum_fusion), channel_id=1, source_target_pairs={{0,1},{1,0},{2,3},{3,2},{4,5},{5,4},{6,7},{7,6},{8,9},{9,8},{10,11... | collective-permute-start | bytes 1572872 | tf_op jit(solution)/shard_map/ppermute | solution.py:23
  118.1 1.5 collective-permute-done.7
  119.6 3.4 %fusion.6 = f32[256,2048]{1,0:T(8,128)S(1)} fusion(bf16[256,1024]{1,0:T(8,128)(2,1)S(1)} %collective-permute-done.7, bf16[1024,2048]{1,0:T(8,128)(2,1)} %collective-permute-done.8), kind=kOutput, calls=%fused_computation.28 | convolution fusion | flops 1073741824 | bytes 6815744 | tf_op jit(solution)/shard_map/dot_general | solution.py:278
  123.1 4.0 %multiply_reduce_fusion = (f32[256]{0:T(256)S(1)}, f32[256,2048]{1,0:T(8,128)S(1)}) fusion(f32[256,2048]{1,0:T(8,128)S(1)} %fusion.6, bf16[1024,2048]{1,0:T(8,128)(2,1)} %constant_dynamic-update-slice_fusion.2, bf16[256,256]{1,0:T(8,128)(2,1)S(1)} %collective-permute-done.2, bf16[256,256]{1,0:T(8,128)(2,1)S(1)} %collective-permute-done.1, ...), kind=kOutput, calls=%fused_computation.6 | convolution fusion | flops 1078460160 | bytes 9962496 | tf_op jit(solution)/shard_map/dot_general | solution.py:277
  127.1 0.0 all-gather.3.cloned.1.call-done
  127.1 4.5 %fusion.2 = f32[256,1408]{1,0:T(8,128)S(1)} fusion(bf16[2048,1408]{1,0:T(8,128)(2,1)} %all-gather.3.cloned.1.call-done, f32[256,2048]{1,0:T(8,128)S(1)} %get-tuple-element.18, f32[2048]{0:T(1024)S(1)} %copy-done.6, f32[256]{0:T(256)S(1)} %add_rsqrt_fusion), kind=kOutput, calls=%fused_computation.7 | convolution fusion | flops 1477967872 | bytes 9315328 | tf_op jit(solution)/shard_map/dot_general | solution.py:282
  131.6 0.3 fusion.5
  132.0 48.4 %all-gather.5.cloned.1.call-done = bf16[704,2048]{0,1:T(8,128)(2,1)} async-done(((bf16[704,64]{0,1:T(8,128)(2,1)}), bf16[704,2048]{0,1:T(8,128)(2,1)}) %all-gather.5.cloned.1.call-update) | async-done | bytes 2883600 | tf_op jit(solution)/shard_map/all_gather | solution.py:219
  180.3 3.2 %convolution_convert_fusion = bf16[128,2048]{1,0:T(8,128)(2,1)S(1)} fusion(bf16[128,704]{1,0:T(8,128)(2,1)S(1)} %bitcast.16, bf16[704,2048]{0,1:T(8,128)(2,1)} %all-gather.5.cloned.1.call-done), kind=kOutput, calls=%fused_computation.2 | convolution fusion | flops 369360896 | bytes 3588096 | tf_op jit(solution)/shard_map/dot_general | solution.py:290
  183.5 4.7 %collective-permute-start.9 = (bf16[128,2048]{1,0:T(8,128)(2,1)S(1)}, bf16[128,2048]{1,0:T(8,128)(2,1)S(1)}, u32[]{:S(2)}, u32[]{:S(2)}) collective-permute-start(bf16[128,2048]{1,0:T(8,128)(2,1)S(1)} %convolution_convert_fusion), channel_id=1, source_target_pairs={{0,1},{1,0},{2,3},{3,2},{4,5},{5,4},{6,7},{7,6},{8,9},{9,8},{10,11... | collective-permute-start | bytes 1572872 | tf_op jit(solution)/shard_map/ppermute | solution.py:23
  188.2 1.5 collective-permute-done.9
  189.7 2.0 add_convert_fusion
  191.7 4.0 %all-to-all-start.2 = ((bf16[4,32,2048]{2,1,0:T(8,128)(2,1)}), bf16[4,32,2048]{2,1,0:T(8,128)(2,1)S(1)}, u32[]{:S(2)}, u32[]{:S(2)}) async-start(bf16[4,32,2048]{2,1,0:T(8,128)(2,1)} %bitcast.5), calls=%async_computation.2 | async-start | bytes 1048576 | tf_op jit(solution)/shard_map/all_to_all | solution.py:294
  195.6 8.9 %all-to-all-done.2 = bf16[4,32,2048]{2,1,0:T(8,128)(2,1)S(1)} async-done(((bf16[4,32,2048]{2,1,0:T(8,128)(2,1)}), bf16[4,32,2048]{2,1,0:T(8,128)(2,1)S(1)}, u32[]{:S(2)}, u32[]{:S(2)}) %all-to-all-start.2) | async-done | bytes 524320 | tf_op jit(solution)/shard_map/all_to_all | solution.py:294
  204.5 0.1 convert_reduce_fusion
  204.6 0.7 add_convert_fusion.1
  (24 shorter events, 0.2 us)
Async XLA Ops:
  6.5 120.6 %all-gather.3.cloned.1.call-start = ((), (), s32[]{:S(2)}) async-start(), calls=%async_computation.3 | async-start | bytes 5947392 | tf_op jit(solution)/shard_map/all_gather | solution.py:216
  8.3 172.0 %all-gather.5.cloned.1.call-start = ((), (), s32[]{:S(2)}) async-start(), calls=%async_computation.4 | async-start | bytes 3244032 | tf_op jit(solution)/shard_map/all_gather | solution.py:219
  12.3 42.0 %copy-start.3 = (bf16[256,64]{0,1:T(8,128)(2,1)S(1)}, bf16[256,64]{0,1:T(8,128)(2,1)}, u32[]{:S(2)}) copy-start(bf16[256,64]{0,1:T(8,128)(2,1)} %param.21) | copy-start | bytes 98308
  12.3 42.8 %copy-start.4 = (bf16[256,64]{0,1:T(8,128)(2,1)S(1)}, bf16[256,64]{0,1:T(8,128)(2,1)}, u32[]{:S(2)}) copy-start(bf16[256,64]{0,1:T(8,128)(2,1)} %param.24) | copy-start | bytes 98308
  12.3 24.1 %collective-permute-start.3 = (bf16[256,2048]{1,0:T(8,128)(2,1)S(1)}, bf16[256,2048]{1,0:T(8,128)(2,1)S(1)}, u32[]{:S(2)}, u32[]{:S(2)}) collective-permute-start(bf16[256,2048]{1,0:T(8,128)(2,1)S(1)} %get-tuple-element.11), channel_id=1, source_target_pairs={{0,2},{2,4},{4,6},{6,0},{1,3},{3,5},{5,7},{7,1},{8,10},{10,12},{12... | collective-permute-start | bytes 3145736 | tf_op jit(solution)/shard_map/ppermute | solution.py:23
  14.4 24.0 %collective-permute-start.4 = (bf16[256,2048]{1,0:T(8,128)(2,1)S(1)}, bf16[256,2048]{1,0:T(8,128)(2,1)S(1)}, u32[]{:S(2)}, u32[]{:S(2)}) collective-permute-start(bf16[256,2048]{1,0:T(8,128)(2,1)S(1)} %get-tuple-element.11), channel_id=1, source_target_pairs={{0,6},{2,0},{4,2},{6,4},{1,7},{3,1},{5,3},{7,5},{8,14},{10,8},{12,... | collective-permute-start | bytes 3145736 | tf_op jit(solution)/shard_map/ppermute | solution.py:23
  36.5 12.6 %collective-permute-start.5 = (bf16[128,2048]{1,0:T(8,128)(2,1)S(1)}, bf16[128,2048]{1,0:T(8,128)(2,1)S(1)}, u32[]{:S(2)}, u32[]{:S(2)}) collective-permute-start(bf16[128,2048]{1,0:T(8,128)(2,1)S(1)} %slice.16), channel_id=1, source_target_pairs={{0,2},{2,4},{4,6},{6,0},{1,3},{3,5},{5,7},{7,1},{8,10},{10,12},{12... | collective-permute-start | bytes 1572872 | tf_op jit(solution)/shard_map/ppermute | solution.py:23
  38.4 51.8 %copy-start.5 = (bf16[256,64]{0,1:T(8,128)(2,1)S(1)}, bf16[256,64]{0,1:T(8,128)(2,1)}, u32[]{:S(2)}) copy-start(bf16[256,64]{0,1:T(8,128)(2,1)} %param.20) | copy-start | bytes 98308
  38.4 11.6 %collective-permute-start.6 = (bf16[128,2048]{1,0:T(8,128)(2,1)S(1)}, bf16[128,2048]{1,0:T(8,128)(2,1)S(1)}, u32[]{:S(2)}, u32[]{:S(2)}) collective-permute-start(bf16[128,2048]{1,0:T(8,128)(2,1)S(1)} %slice.17), channel_id=1, source_target_pairs={{0,6},{2,0},{4,2},{6,4},{1,7},{3,1},{5,3},{7,5},{8,14},{10,8},{12,... | collective-permute-start | bytes 1572872 | tf_op jit(solution)/shard_map/ppermute | solution.py:23
  50.8 68.8 %collective-permute-start.8 = (bf16[1024,2048]{1,0:T(8,128)(2,1)}, bf16[1024,2048]{1,0:T(8,128)(2,1)}, u32[]{:S(2)}, u32[]{:S(2)}) collective-permute-start(bf16[1024,2048]{1,0:T(8,128)(2,1)} %constant_dynamic-update-slice_fusion.2), channel_id=1, source_target_pairs={{0,1},{1,0},{2,3},{3,2},{4,5},{5,4},{6,7},{7,6},{8,9},{9,8},{10,11... | collective-permute-start | bytes 12582920 | tf_op jit(solution)/shard_map/ppermute | solution.py:23
  86.2 14.8 %all-to-all-start.1 = ((bf16[32,16,128]{2,1,0:T(8,128)(2,1)}), bf16[32,16,128]{2,1,0:T(8,128)(2,1)S(1)}, u32[]{:S(2)}, u32[]{:S(2)}) async-start(bf16[32,16,128]{2,1,0:T(8,128)(2,1)} %shard_map.183), calls=%async_computation.1 | async-start | bytes 262144 | tf_op jit(solution)/shard_map/all_to_all | solution.py:259
  101.1 0.7 copy-start.1
  103.8 19.2 %copy-start.2 = (bf16[256,256]{1,0:T(8,128)(2,1)S(1)}, bf16[256,256]{1,0:T(8,128)(2,1)}, u32[]{:S(2)}) copy-start(bf16[256,256]{1,0:T(8,128)(2,1)} %shard_map.184) | copy-start | bytes 393220
  103.8 5.2 %collective-permute-start = (bf16[256,256]{1,0:T(8,128)(2,1)}, bf16[256,256]{1,0:T(8,128)(2,1)S(1)}, u32[]{:S(2)}, u32[]{:S(2)}) collective-permute-start(bf16[256,256]{1,0:T(8,128)(2,1)} %shard_map.184), channel_id=1, source_target_pairs={{0,2},{2,4},{4,6},{6,0},{1,3},{3,5},{5,7},{7,1},{8,10},{10,12},{12... | collective-permute-start | bytes 393224 | tf_op jit(solution)/shard_map/ppermute | solution.py:23
  103.8 5.2 %collective-permute-start.1 = (bf16[256,256]{1,0:T(8,128)(2,1)}, bf16[256,256]{1,0:T(8,128)(2,1)S(1)}, u32[]{:S(2)}, u32[]{:S(2)}) collective-permute-start(bf16[256,256]{1,0:T(8,128)(2,1)} %shard_map.184), channel_id=1, source_target_pairs={{0,6},{2,0},{4,2},{6,4},{1,7},{3,1},{5,3},{7,5},{8,14},{10,8},{12,... | collective-permute-start | bytes 393224 | tf_op jit(solution)/shard_map/ppermute | solution.py:23
  106.5 5.8 %collective-permute-start.2 = (bf16[256,256]{1,0:T(8,128)(2,1)}, bf16[256,256]{1,0:T(8,128)(2,1)S(1)}, u32[]{:S(2)}, u32[]{:S(2)}) collective-permute-start(bf16[256,256]{1,0:T(8,128)(2,1)} %shard_map.184), channel_id=1, source_target_pairs={{0,4},{2,6},{4,0},{6,2},{1,5},{3,7},{5,1},{7,3},{8,12},{10,14},{12... | collective-permute-start | bytes 393224 | tf_op jit(solution)/shard_map/ppermute | solution.py:23
  113.2 6.4 %collective-permute-start.7 = (bf16[256,1024]{1,0:T(8,128)(2,1)S(1)}, bf16[256,1024]{1,0:T(8,128)(2,1)S(1)}, u32[]{:S(2)}, u32[]{:S(2)}) collective-permute-start(bf16[256,1024]{1,0:T(8,128)(2,1)S(1)} %pad_maximum_fusion), channel_id=1, source_target_pairs={{0,1},{1,0},{2,3},{3,2},{4,5},{5,4},{6,7},{7,6},{8,9},{9,8},{10,11... | collective-permute-start | bytes 1572872 | tf_op jit(solution)/shard_map/ppermute | solution.py:23
  123.1 4.0 %copy-start.6 = (f32[2048]{0:T(1024)S(1)}, f32[2048]{0:T(1024)}, u32[]{:S(2)}) copy-start(f32[2048]{0:T(1024)} %param.34) | copy-start | bytes 24580
  180.3 9.4 %copy-start = (bf16[704,2048]{0,1:T(8,128)(2,1)S(1)}, bf16[704,2048]{0,1:T(8,128)(2,1)}, u32[]{:S(2)}) copy-start(bf16[704,2048]{0,1:T(8,128)(2,1)} %all-gather.5.cloned.1.call-done) | copy-start | bytes 8650756
  183.5 6.2 %collective-permute-start.9 = (bf16[128,2048]{1,0:T(8,128)(2,1)S(1)}, bf16[128,2048]{1,0:T(8,128)(2,1)S(1)}, u32[]{:S(2)}, u32[]{:S(2)}) collective-permute-start(bf16[128,2048]{1,0:T(8,128)(2,1)S(1)} %convolution_convert_fusion), channel_id=1, source_target_pairs={{0,1},{1,0},{2,3},{3,2},{4,5},{5,4},{6,7},{7,6},{8,9},{9,8},{10,11... | collective-permute-start | bytes 1572872 | tf_op jit(solution)/shard_map/ppermute | solution.py:23
  191.7 12.9 %all-to-all-start.2 = ((bf16[4,32,2048]{2,1,0:T(8,128)(2,1)}), bf16[4,32,2048]{2,1,0:T(8,128)(2,1)S(1)}, u32[]{:S(2)}, u32[]{:S(2)}) async-start(bf16[4,32,2048]{2,1,0:T(8,128)(2,1)} %bitcast.5), calls=%async_computation.2 | async-start | bytes 1048576 | tf_op jit(solution)/shard_map/all_to_all | solution.py:294
Sparse Core Ops, SparseCore 0:
  9.9 93.2 all-gather.2
  105.8 74.5 all-gather.4
